TPU v7x, 32 devices: a whole 2x2x4 slice. The times are simulated.
32 devices in a mesh: sp: 8 (over z, y), tp: 4 (over x, core).
Axes of the slice: x: 2, y: 2, z: 4, core: 2. Of those that a mesh axis runs over, the one named last changes fastest.
Arguments:
- stream: bfloat16 [4096, 2048], P(('sp', 'tp')), may hold values from -6 to 6
- conv_in_a: bfloat16 [4096, 1024], P('sp', 'tp'), may hold values from -6 to 6
- conv_in_b: bfloat16 [4096, 1024], P('sp', 'tp'), may hold values from -6 to 6
- gate_in_a: bfloat16 [4096, 1024], P('sp', 'tp'), may hold values from -6 to 6
- gate_in_b: bfloat16 [4096, 1024], P('sp', 'tp'), may hold values from -6 to 6
- conv_w_a: bfloat16 [4, 1024], P(None, 'tp'), may hold values from -3 to 3
- conv_w_b: bfloat16 [4, 1024], P(None, 'tp'), may hold values from -3 to 3
- rec_gate_a: bfloat16 [16, 64, 64], P('tp'), may hold values from -0.75 to 0.75
- inp_gate_a: bfloat16 [16, 64, 64], P('tp'), may hold values from -0.75 to 0.75
- rec_gate_b: bfloat16 [8, 128, 128], P('tp'), may hold values from -0.5 to 0.5
- inp_gate_b: bfloat16 [8, 128, 128], P('tp'), may hold values from -0.5 to 0.5
- decay_a: float32 [1024], P('tp'), may hold values from 3 to 20
- decay_b: float32 [1024], P('tp'), may hold values from 3 to 20
- decay_increments: float32 [4096], P('sp'), may hold values from -0.7 to 0
- out_w_a: bfloat16 [1024, 2048], P('tp'), may hold values from -0.5 to 0.5
- out_w_b: bfloat16 [1024, 2048], P('tp'), may hold values from -0.5 to 0.5
- norm_gain: bfloat16 [2048], replicated, may hold values from 0.099609375 to 1.8984375
- expert_ids: int32 [4096, 2], P(('sp', 'tp')), may hold values from 0 to 31, as said below
- group_prob: float32 [4096], P(('sp', 'tp')), may hold values from 0.3 to 1
- pick_gap: float32 [4096], P(('sp', 'tp')), may hold values from -6 to 6
- w_gate: bfloat16 [32, 2048, 1024], P(('sp', 'tp')), may hold values from -0.125 to 0.125
- w_up: bfloat16 [32, 2048, 1024], P(('sp', 'tp')), may hold values from -0.125 to 0.125
- w_down: bfloat16 [32, 1024, 2048], P(('sp', 'tp')), may hold values from -0.5 to 0.5
Outputs:
- result: bfloat16 [4096, 2048], P(('sp', 'tp'))
Inputs may be any that keep to these rules, and one draw needn't show every extreme that they name: `expert_ids`: each row names two different experts of one group: both lie in g * 8 to g * 8 + 7 for some g. In each aligned block of 128 rows no expert is named more than 16 times, and in every block some expert is named exactly 16 times.
All inputs are finite; a program needn't handle non-finite values.
Results may differ from a plain program's by a relative error of at most 0.015.
Values may be sent and summed in bfloat16 or wider, within the bound.
A program may use at most 128 MiB of HBM per device.

v0:
```python
import jax
import jax.numpy as jnp
from jax import lax
from jax.sharding import PartitionSpec as P

EPSILON = 1e-06
GATE_SCALE = 8.0


def from_behind(array, axis, by):
    size = lax.axis_size(axis)
    pairs = [(i, i + by) for i in range(size) if 0 <= i + by < size]
    return lax.ppermute(array, axis, pairs)


def prefix(value, axis, join, neutral):
    count, mine = (lax.axis_size(axis), lax.axis_index(axis))
    pieces = jax.tree.map(lambda part: lax.all_gather(part, axis), value)
    running = jax.tree.map(
        lambda part, zero: jnp.full_like(part, 0) + jnp.asarray(zero, part.dtype), value, neutral
    )

    def step(position, running):
        longer = join(running, jax.tree.map(lambda part: part[position], pieces))
        return jax.tree.map(lambda new, old: jnp.where(position < mine, new, old), longer, running)

    return lax.fori_loop(0, count - 1, step, running)


def causal_taps(source, tail_rows, weights):
    length = source.shape[0]
    tap_count = weights.shape[0]
    rim_count = tail_rows.shape[0]
    row_index = jnp.arange(length, dtype=jnp.int32)[:, None]
    own_index = jnp.arange(length, dtype=jnp.int32)[None, :]
    rim_index = jnp.arange(rim_count, dtype=jnp.int32)[None, :]
    total = weights[tap_count - 1].astype(jnp.float32)[None, :] * source.astype(jnp.float32)
    for offset in range(tap_count - 1):
        lag = tap_count - 1 - offset
        own_shift = (row_index - own_index == lag).astype(jnp.bfloat16)
        rim_shift = (rim_index == rim_count + row_index - lag).astype(jnp.bfloat16)
        moved = jnp.dot(own_shift, source, preferred_element_type=jnp.float32)
        moved = moved + jnp.dot(rim_shift, tail_rows, preferred_element_type=jnp.float32)
        total = total + weights[offset].astype(jnp.float32)[None, :] * moved
    return total.astype(jnp.bfloat16)


def recurrence_inputs(conv_out, rec_gate, inp_gate, decay, jump_log):
    length = conv_out.shape[0]
    head_count = rec_gate.shape[0]
    head_dim = rec_gate.shape[1]
    blocks = conv_out.reshape(length, head_count, head_dim)
    recur = jax.nn.sigmoid(
        jnp.einsum("thi,hij->thj", blocks, rec_gate, preferred_element_type=jnp.float32).reshape(
            length, -1
        )
    )
    admit = jax.nn.sigmoid(
        jnp.einsum("thi,hij->thj", blocks, inp_gate, preferred_element_type=jnp.float32).reshape(
            length, -1
        )
    )
    log_decay = -GATE_SCALE * recur * jax.nn.softplus(-decay)[None, :] + jump_log[:, None]
    drive = jnp.sqrt(-jnp.expm1(2.0 * log_decay)) * admit * conv_out.astype(jnp.float32)
    return (log_decay, drive)


def link_states(earlier, later):
    return (earlier[0] * later[0], later[0] * earlier[1] + later[1])


def local_recurrence(log_decay, drives):
    length, channel_count = log_decay.shape
    span = min(128, length)
    block_count = length // span
    lower = jnp.arange(span, dtype=jnp.int32)[:, None] >= jnp.arange(span, dtype=jnp.int32)[None, :]
    cumulative = jnp.einsum(
        "ts,bsc->btc",
        lower.astype(jnp.float32),
        log_decay.reshape(block_count, span, channel_count),
        precision=lax.Precision.HIGHEST,
    )
    drive_blocks = drives.reshape(block_count, span, channel_count)

    def block_states(operands):
        cum_block, drive_block = operands
        spread = jnp.minimum(cum_block[:, None, :] - cum_block[None, :, :], 0.0)
        weight = jnp.where(lower[:, :, None], jnp.exp(spread), 0.0)
        return jnp.sum(weight * drive_block[None, :, :], axis=1)

    inner_states = lax.map(block_states, (cumulative, drive_blocks))
    within_factor = jnp.exp(cumulative)

    def link_blocks(carry, operands):
        factor_end, state_end = operands
        carry_factor, carry_state = carry
        following = (carry_factor * factor_end, factor_end * carry_state + state_end)
        return (following, carry)

    start_pair = (jnp.ones((channel_count,), jnp.float32), jnp.zeros((channel_count,), jnp.float32))
    last_pair, entering = lax.scan(
        link_blocks, start_pair, (within_factor[:, -1], inner_states[:, -1])
    )
    states = inner_states + within_factor * entering[1][:, None, :]
    running_factor = within_factor * entering[0][:, None, :]
    return (running_factor.reshape(length, channel_count), states.reshape(length, channel_count))


def shards(
    stream,
    conv_in_a,
    conv_in_b,
    gate_in_a,
    gate_in_b,
    conv_w_a,
    conv_w_b,
    rec_gate_a,
    inp_gate_a,
    rec_gate_b,
    inp_gate_b,
    decay_a,
    decay_b,
    decay_increments,
    out_w_a,
    out_w_b,
    norm_gain,
    expert_ids,
    group_prob,
    pick_gap,
    w_gate,
    w_up,
    w_down,
):
    tap_count = conv_w_a.shape[0]
    length = conv_in_a.shape[0]
    tail_a, tail_b = from_behind(
        (conv_in_a[length - tap_count + 1 :], conv_in_b[length - tap_count + 1 :]), "sp", 1
    )
    conv_a = causal_taps(conv_in_a, tail_a, conv_w_a)
    conv_b = causal_taps(conv_in_b, tail_b, conv_w_b)
    log_a, drive_a = recurrence_inputs(conv_a, rec_gate_a, inp_gate_a, decay_a, decay_increments)
    log_b, drive_b = recurrence_inputs(conv_b, rec_gate_b, inp_gate_b, decay_b, decay_increments)
    log_all = jnp.concatenate([log_a, log_b], axis=1)
    drives = jnp.concatenate([drive_a, drive_b], axis=1)
    running_factor, local_states = local_recurrence(log_all, drives)
    channel_count = log_all.shape[1]
    identity_pair = (
        jnp.ones((channel_count,), jnp.float32),
        jnp.zeros((channel_count,), jnp.float32),
    )
    incoming_factor, carried = prefix(
        (running_factor[-1], local_states[-1]), "sp", link_states, identity_pair
    )
    states = local_states + running_factor * carried[None, :]
    width_a = conv_in_a.shape[1]
    hidden_a = (states[:, :width_a] * jax.nn.gelu(gate_in_a.astype(jnp.float32))).astype(
        jnp.bfloat16
    )
    hidden_b = (states[:, width_a:] * jax.nn.gelu(gate_in_b.astype(jnp.float32))).astype(
        jnp.bfloat16
    )
    tp_count = lax.axis_size("tp")
    row_count = length // tp_count
    whole_a, whole_b = (
        lax.all_to_all(hidden_a, "tp", split_axis=0, concat_axis=1, tiled=True),
        lax.all_to_all(hidden_b, "tp", split_axis=0, concat_axis=1, tiled=True),
    )
    total = jnp.dot(
        whole_a,
        lax.all_gather(out_w_a, "tp", axis=0, tiled=True),
        preferred_element_type=jnp.float32,
    )
    mixed_rows = total + jnp.dot(
        whole_b,
        lax.all_gather(out_w_b, "tp", axis=0, tiled=True),
        preferred_element_type=jnp.float32,
    )
    middle = (stream.astype(jnp.float32) + mixed_rows).astype(jnp.bfloat16)
    middle_f = middle.astype(jnp.float32)
    scale_rows = lax.rsqrt(jnp.mean(middle_f * middle_f, axis=-1, keepdims=True) + EPSILON)
    normed = (middle_f * scale_rows * norm_gain.astype(jnp.float32)[None, :]).astype(jnp.bfloat16)
    width = normed.shape[1]
    sequence_parallel_count = lax.axis_size("sp")
    experts = sequence_parallel_count * tp_count * w_gate.shape[0]
    slot_count = 4 * row_count // experts
    flat_ids = expert_ids.reshape(-1)
    onehot = (flat_ids[:, None] == jnp.arange(experts, dtype=jnp.int32)[None, :]).astype(jnp.int32)
    ranks = jnp.sum(jnp.cumsum(onehot, axis=0) * onehot, axis=1) - 1
    destination = flat_ids * slot_count + ranks
    copies = jnp.repeat(normed, expert_ids.shape[1], axis=0)
    buffer = jnp.zeros((experts * slot_count, width), jnp.bfloat16).at[destination].set(copies)
    buffer = buffer.reshape(experts, slot_count, width)
    arrived = lax.all_to_all(buffer, ("sp", "tp"), split_axis=0, concat_axis=0, tiled=True)
    flat_rows = arrived.reshape(-1, arrived.shape[-1])
    gate_part = jnp.dot(flat_rows, w_gate[0], preferred_element_type=jnp.float32)
    up_part = jnp.dot(flat_rows, w_up[0], preferred_element_type=jnp.float32)
    inner = (jax.nn.silu(gate_part) * up_part).astype(jnp.bfloat16)
    served = jnp.dot(inner, w_down[0], preferred_element_type=jnp.float32).astype(jnp.bfloat16)
    returned = lax.all_to_all(
        served.reshape(arrived.shape), ("sp", "tp"), split_axis=0, concat_axis=0, tiled=True
    )
    returned = returned.reshape(experts * slot_count, width)
    picked = returned[destination].reshape(row_count, expert_ids.shape[1], width)
    first_weight = group_prob * jax.nn.sigmoid(pick_gap)
    second_weight = group_prob * jax.nn.sigmoid(-pick_gap)
    total = (
        middle_f
        + first_weight[:, None] * picked[:, 0].astype(jnp.float32)
        + second_weight[:, None] * picked[:, 1].astype(jnp.float32)
    )
    return total.astype(jnp.bfloat16)


def solution(mesh):
    placed = (
        P(("sp", "tp"), None),
        P("sp", "tp"),
        P("sp", "tp"),
        P("sp", "tp"),
        P("sp", "tp"),
        P(None, "tp"),
        P(None, "tp"),
        P("tp", None, None),
        P("tp", None, None),
        P("tp", None, None),
        P("tp", None, None),
        P("tp"),
        P("tp"),
        P("sp"),
        P("tp", None),
        P("tp", None),
        P(),
        P(("sp", "tp"), None),
        P(("sp", "tp")),
        P(("sp", "tp")),
        P(("sp", "tp"), None, None),
        P(("sp", "tp"), None, None),
        P(("sp", "tp"), None, None),
    )
    return jax.shard_map(
        shards, mesh=mesh, in_specs=placed, out_specs=P(("sp", "tp"), None), check_vma=False
    )
```

profile of v0, /device:TPU:0, one launch (start us, length us, event | category | flops | bytes accessed | tf_op | source)
XLA Modules:
  0.0 302.9 jit_solution(16909540413028854363)
XLA Ops:
  6.6 0.7 all-gather.5.cloned.1.call-update
  7.4 0.7 slice.62
  8.1 4.9 %collective-permute-start = (bf16[3,256]{1,0:T(4,128)(2,1)S(1)}, bf16[3,256]{1,0:T(4,128)(2,1)S(1)}, u32[]{:S(2)}, u32[]{:S(2)}) collective-permute-start(bf16[3,256]{1,0:T(4,128)(2,1)S(1)} %slice.62), channel_id=1, source_target_pairs={{0,4},{4,8},{8,12},{12,16},{16,20},{20,24},{24,28},{1,5},{5,9},{9,... | collective-permute-start | bytes 4616 | tf_op jit(solution)/shard_map/ppermute | solution.py:13
  12.9 0.7 slice.67
  13.6 3.5 %collective-permute-start.1 = (bf16[3,256]{1,0:T(4,128)(2,1)S(1)}, bf16[3,256]{1,0:T(4,128)(2,1)S(1)}, u32[]{:S(2)}, u32[]{:S(2)}) collective-permute-start(bf16[3,256]{1,0:T(4,128)(2,1)S(1)} %slice.67), channel_id=1, source_target_pairs={{0,4},{4,8},{8,12},{12,16},{16,20},{20,24},{24,28},{1,5},{5,9},{9,... | collective-permute-start | bytes 4616 | tf_op jit(solution)/shard_map/ppermute | solution.py:13
  17.2 2.1 fusion.55
  19.4 2.2 fusion.59
  21.5 2.1 fusion.63
  23.6 0.3 fusion.53
  24.0 1.1 fusion.57
  25.1 0.3 fusion.61
  25.9 0.6 reduce-window.6
  26.5 0.2 slice_reduce_fusion
  27.6 1.3 fusion.31
  28.9 1.4 fusion.29
  30.3 1.4 fusion.40
  31.8 0.3 fusion.33
  32.1 0.3 fusion.37
  32.5 0.3 fusion.24
  32.8 0.3 fusion.22
  33.2 0.4 fusion.41
  33.5 0.3 fusion.35
  33.9 0.3 fusion.39
  34.3 0.8 fusion.87
  35.2 0.3 copy.120
  35.5 1.2 div.51
  36.7 0.2 copy.100
  37.0 1.2 div.49
  38.2 1.0 copy.96
  39.2 1.2 multiply_add_fusion.4
  40.4 1.8 fusion.120
  42.2 39.6 %while.42 = (s32[]{:T(128)}, f32[4,128,512]{2,1,0:T(8,128)S(1)}, f32[4,128,512]{2,1,0:T(8,128)S(1)}, f32[4,128,512]{2,1,0:T(8,128)S(1)}, s32[]{:T(128)}) while((s32[]{:T(128)}, f32[4,128,512]{2,1,0:T(8,128)S(1)}, f32[4,128,512]{2,1,0:T(8,128)S(1)}, f32[4,128,512]{2,1,0:T(8,128)S(1)}, s32[]{:T(128)}) %tuple.113), condition=%wide.region_2.3_spmd.clone, body=%wide.region_0.2_spmd.clone.sunk | while | flops 41893888 | bytes 2392133 | solution.py:91
  42.3 9.8 %multiply_reduce_fusion.3 = f32[128,512]{1,0:T(8,128)S(1)} fusion(f32[128,512]{1,0:T(8,128)S(1)} %get-tuple-element.407, f32[128,512]{1,0:T(8,128)S(1)} %get-tuple-element.408, pred[128,128]{1,0:T(8,128)(4,1)S(1)} %iota_compare_fusion.14), kind=kLoop, calls=%fused_computation.3.clone.1 | loop fusion | flops 41877504 | bytes 802816 | tf_op jit(solution)/shard_map/while/body/eval_jaxpr/reduce_sum | solution.py:89
  52.2 9.8 %multiply_reduce_fusion.3 = f32[128,512]{1,0:T(8,128)S(1)} fusion(f32[128,512]{1,0:T(8,128)S(1)} %get-tuple-element.407, f32[128,512]{1,0:T(8,128)S(1)} %get-tuple-element.408, pred[128,128]{1,0:T(8,128)(4,1)S(1)} %iota_compare_fusion.14), kind=kLoop, calls=%fused_computation.3.clone.1 | loop fusion | flops 41877504 | bytes 802816 | tf_op jit(solution)/shard_map/while/body/eval_jaxpr/reduce_sum | solution.py:89
  62.1 9.8 %multiply_reduce_fusion.3 = f32[128,512]{1,0:T(8,128)S(1)} fusion(f32[128,512]{1,0:T(8,128)S(1)} %get-tuple-element.407, f32[128,512]{1,0:T(8,128)S(1)} %get-tuple-element.408, pred[128,128]{1,0:T(8,128)(4,1)S(1)} %iota_compare_fusion.14), kind=kLoop, calls=%fused_computation.3.clone.1 | loop fusion | flops 41877504 | bytes 802816 | tf_op jit(solution)/shard_map/while/body/eval_jaxpr/reduce_sum | solution.py:89
  72.0 9.8 %multiply_reduce_fusion.3 = f32[128,512]{1,0:T(8,128)S(1)} fusion(f32[128,512]{1,0:T(8,128)S(1)} %get-tuple-element.407, f32[128,512]{1,0:T(8,128)S(1)} %get-tuple-element.408, pred[128,128]{1,0:T(8,128)(4,1)S(1)} %iota_compare_fusion.14), kind=kLoop, calls=%fused_computation.3.clone.1 | loop fusion | flops 41877504 | bytes 802816 | tf_op jit(solution)/shard_map/while/body/eval_jaxpr/reduce_sum | solution.py:89
  81.9 0.7 copy.105
  82.6 0.9 slice.82
  83.5 0.6 while.43
  84.1 1.6 multiply_add_fusion.2
  85.8 26.1 %all-gather.1 = f32[8,1,512]{2,1,0:T(1,128)S(1)} all-gather(f32[1,1,512]{2,1,0:T(1,128)S(1)} %slice_bitcast_fusion.1), channel_id=1, replica_groups=mesh['sp'=8,'tp'=4] {'sp'}, dimensions={0}, use_global_device_ids=true | all-gather | bytes 18432 | tf_op jit(solution)/shard_map/all_gather | solution.py:18
  111.9 26.1 %all-gather = f32[8,1,512]{2,1,0:T(1,128)S(1)} all-gather(f32[1,1,512]{2,1,0:T(1,128)S(1)} %slice_bitcast_fusion.2), channel_id=1, replica_groups=mesh['sp'=8,'tp'=4] {'sp'}, dimensions={0}, use_global_device_ids=true | all-gather | bytes 18432 | tf_op jit(solution)/shard_map/all_gather | solution.py:18
  138.0 0.4 while.44
  138.4 0.2 multiply_add_fusion.1
  138.6 2.2 fusion.80
  140.8 3.5 %all-to-all-start = ((bf16[4,128,256]{2,1,0:T(8,128)(2,1)}), bf16[4,128,256]{2,1,0:T(8,128)(2,1)S(1)}, u32[]{:S(2)}, u32[]{:S(2)}) async-start(bf16[4,128,256]{2,1,0:T(8,128)(2,1)} %bitcast.27), calls=%async_computation | async-start | bytes 524288 | tf_op jit(solution)/shard_map/all_to_all | solution.py:165
  144.3 6.0 %all-to-all-done = bf16[4,128,256]{2,1,0:T(8,128)(2,1)S(1)} async-done(((bf16[4,128,256]{2,1,0:T(8,128)(2,1)}), bf16[4,128,256]{2,1,0:T(8,128)(2,1)S(1)}, u32[]{:S(2)}, u32[]{:S(2)}) %all-to-all-start) | async-done | bytes 262176 | tf_op jit(solution)/shard_map/all_to_all | solution.py:165
  150.3 3.6 %all-to-all-start.1 = ((bf16[4,128,256]{2,1,0:T(8,128)(2,1)}), bf16[4,128,256]{2,1,0:T(8,128)(2,1)S(1)}, u32[]{:S(2)}, u32[]{:S(2)}) async-start(bf16[4,128,256]{2,1,0:T(8,128)(2,1)} %bitcast.30), calls=%async_computation.1 | async-start | bytes 524288 | tf_op jit(solution)/shard_map/all_to_all | solution.py:166
  154.1 5.8 %all-to-all-done.1 = bf16[4,128,256]{2,1,0:T(8,128)(2,1)S(1)} async-done(((bf16[4,128,256]{2,1,0:T(8,128)(2,1)}), bf16[4,128,256]{2,1,0:T(8,128)(2,1)S(1)}, u32[]{:S(2)}, u32[]{:S(2)}) %all-to-all-start.1) | async-done | bytes 262176 | tf_op jit(solution)/shard_map/all_to_all | solution.py:166
  160.1 2.9 fusion.121
  163.0 3.0 %multiply_reduce_fusion.1 = (f32[128]{0:T(128)S(1)}, f32[128,2048]{1,0:T(8,128)S(1)}) fusion(f32[128,2048]{1,0:T(8,128)S(1)} %fusion.121, bf16[128,1024]{0,1:T(8,128)(2,1)S(1)} %bitcast.202, bf16[1024,2048]{1,0:T(8,128)(2,1)} %all-gather.7.cloned.1.call-done, bf16[128,2048]{1,0:T(8,128)(2,1)S(1)} %copy-done.6), kind=kOutput, calls=%fused_computation.75 | convolution fusion | flops 538705792 | bytes 7078400 | tf_op jit(solution)/shard_map/dot_general | solution.py:173
  166.3 0.6 broadcast_in_dim.26
  166.9 1.2 reshape.224
  168.1 3.5 %scatter_custom_fusion = bf16[512,2048]{1,0:T(8,128)(2,1)S(1)} fusion(s32[256]{0:T(256)S(1)} %bitcast.224, bf16[256,2048]{1,0:T(8,128)(2,1)} %reshape.224, bf16[]{:T(256)} %constant.106.clone.1), kind=kCustom, calls=%fused_computation.76 | custom fusion | bytes 2097664 | tf_op jit(solution)/shard_map/scatter | solution.py:191
  171.7 50.7 %all_to_all.48 = bf16[32,16,2048]{2,1,0:T(8,128)(2,1)S(1)} all-to-all(bf16[32,16,2048]{2,1,0:T(8,128)(2,1)S(1)} %bitcast.193), channel_id=1, replica_groups=mesh['sp'=8,'tp'=4] {'sp','tp'}, dimensions={0} | all-to-all | bytes 4194304 | tf_op jit(solution)/shard_map/all_to_all | solution.py:193
  222.3 1.3 copy-done.3
  223.7 2.3 fusion.6
  226.0 10.0 %fusion.8 = bf16[512,2048]{1,0:T(8,128)(2,1)} fusion(bf16[1,1024,2048]{2,1,0:T(8,128)(2,1)} %param.51, f32[512,1024]{1,0:T(8,128)S(1)} %fusion.6, bf16[512,2048]{1,0:T(8,128)(2,1)} %bitcast.199, bf16[1,2048,1024]{2,1,0:T(8,128)(2,1)} %param.50), kind=kOutput, calls=%fused_computation.22 | convolution fusion | flops 4299161600 | bytes 14680064 | tf_op jit(solution)/shard_map/dot_general | solution.py:198
  236.0 3.8 %all-to-all-start.3 = ((bf16[32,16,2048]{2,1,0:T(8,128)(2,1)}), bf16[32,16,2048]{2,1,0:T(8,128)(2,1)S(1)}, u32[]{:S(2)}, u32[]{:S(2)}) async-start(bf16[32,16,2048]{2,1,0:T(8,128)(2,1)} %bitcast.197), calls=%async_computation.3 | async-start | bytes 4194304 | tf_op jit(solution)/shard_map/all_to_all | solution.py:199
  239.9 48.6 %all-to-all-done.3 = bf16[32,16,2048]{2,1,0:T(8,128)(2,1)S(1)} async-done(((bf16[32,16,2048]{2,1,0:T(8,128)(2,1)}), bf16[32,16,2048]{2,1,0:T(8,128)(2,1)S(1)}, u32[]{:S(2)}, u32[]{:S(2)}) %all-to-all-start.3) | async-done | bytes 2097184 | tf_op jit(solution)/shard_map/all_to_all | solution.py:199
  288.5 2.3 gather_fusion
  290.8 1.8 reshape.201
  292.6 1.5 fusion.119
  294.1 1.9 fusion.46
  (135 shorter events, 3.0 us)
Async XLA Ops:
  6.5 25.2 %copy-start = (bf16[4,64,64]{2,1,0:T(8,128)(2,1)S(1)}, bf16[4,64,64]{2,1,0:T(8,128)(2,1)}, u32[]{:S(2)}) copy-start(bf16[4,64,64]{2,1,0:T(8,128)(2,1)} %param.36) | copy-start | bytes 98308
  6.5 17.1 %copy-start.9 = (bf16[512,256]{1,0:T(8,128)(2,1)S(1)}, bf16[512,256]{1,0:T(8,128)(2,1)}, u32[]{:S(2)}) copy-start(bf16[512,256]{1,0:T(8,128)(2,1)} %param.31) | copy-start | bytes 786436
  6.5 20.4 %copy-start.8 = (bf16[512,256]{1,0:T(8,128)(2,1)S(1)}, bf16[512,256]{1,0:T(8,128)(2,1)}, u32[]{:S(2)}) copy-start(bf16[512,256]{1,0:T(8,128)(2,1)} %param.30) | copy-start | bytes 786436
  6.5 18.9 %copy-start.14 = (s32[128,2]{0,1:T(2,128)S(1)}, s32[128,2]{0,1:T(2,128)}, u32[]{:S(2)}) copy-start(s32[128,2]{0,1:T(2,128)} %param.46) | copy-start | bytes 3076
  6.5 19.3 %copy-start.11 = (bf16[4,256]{1,0:T(4,128)(2,1)S(1)}, bf16[4,256]{1,0:T(4,128)(2,1)}, u32[]{:S(2)}) copy-start(bf16[4,256]{1,0:T(4,128)(2,1)} %param.34) | copy-start | bytes 6148
  6.5 19.4 %copy-start.12 = (bf16[4,256]{1,0:T(4,128)(2,1)S(1)}, bf16[4,256]{1,0:T(4,128)(2,1)}, u32[]{:S(2)}) copy-start(bf16[4,256]{1,0:T(4,128)(2,1)} %param.35) | copy-start | bytes 6148
  6.6 20.2 %copy-start.16 = (f32[256]{0:T(256)S(1)}, f32[256]{0:T(256)}, u32[]{:S(2)}) copy-start(f32[256]{0:T(256)} %param.40) | copy-start | bytes 3076
  6.6 20.2 %copy-start.17 = (f32[256]{0:T(256)S(1)}, f32[256]{0:T(256)}, u32[]{:S(2)}) copy-start(f32[256]{0:T(256)} %param.41) | copy-start | bytes 3076
  6.6 153.5 %all-gather.5.cloned.1.call-start = ((), (), s32[]{:S(2)}) async-start(), calls=%async_computation.4 | async-start | bytes 5242880 | tf_op jit(solution)/shard_map/all_gather | solution.py:170
  7.3 155.7 %all-gather.7.cloned.1.call-start = ((), (), s32[]{:S(2)}) async-start(), calls=%async_computation.5 | async-start | bytes 5242880 | tf_op jit(solution)/shard_map/all_gather | solution.py:175
  8.1 19.5 %collective-permute-start = (bf16[3,256]{1,0:T(4,128)(2,1)S(1)}, bf16[3,256]{1,0:T(4,128)(2,1)S(1)}, u32[]{:S(2)}, u32[]{:S(2)}) collective-permute-start(bf16[3,256]{1,0:T(4,128)(2,1)S(1)} %slice.62), channel_id=1, source_target_pairs={{0,4},{4,8},{8,12},{12,16},{16,20},{20,24},{24,28},{1,5},{5,9},{9,... | collective-permute-start | bytes 4616 | tf_op jit(solution)/shard_map/ppermute | solution.py:13
  13.6 13.6 %copy-start.15 = (bf16[2048]{0:T(1024)(128)(2,1)S(1)}, bf16[2048]{0:T(1024)(128)(2,1)}, u32[]{:S(2)}) copy-start(bf16[2048]{0:T(1024)(128)(2,1)} %param.45) | copy-start | bytes 12292
  13.6 18.9 %collective-permute-start.1 = (bf16[3,256]{1,0:T(4,128)(2,1)S(1)}, bf16[3,256]{1,0:T(4,128)(2,1)S(1)}, u32[]{:S(2)}, u32[]{:S(2)}) collective-permute-start(bf16[3,256]{1,0:T(4,128)(2,1)S(1)} %slice.67), channel_id=1, source_target_pairs={{0,4},{4,8},{8,12},{12,16},{16,20},{20,24},{24,28},{1,5},{5,9},{9,... | collective-permute-start | bytes 4616 | tf_op jit(solution)/shard_map/ppermute | solution.py:13
  25.5 6.6 %copy-start.21 = (bf16[4,64,64]{2,1,0:T(8,128)(2,1)S(1)}, bf16[4,64,64]{2,1,0:T(8,128)(2,1)}, u32[]{:S(2)}) copy-start(bf16[4,64,64]{2,1,0:T(8,128)(2,1)} %param.37) | copy-start | bytes 98308
  28.9 3.9 %copy-start.7 = (f32[512,256]{0,1:T(8,128)S(1)}, f32[512,256]{0,1:T(8,128)}, u32[]{:S(2)}) copy-start(f32[512,256]{0,1:T(8,128)} %fusion.57) | copy-start | bytes 1572868
  31.7 1.8 copy-start.22
  32.1 2.1 copy-start.4
  32.1 1.7 copy-start.23
  32.5 1.7 copy-start.13
  33.9 1.2 copy-start.5
  81.9 2.3 copy-start.2
  82.6 56.1 %copy-start.10 = (bf16[512,256]{1,0:T(8,128)(2,1)S(1)}, bf16[512,256]{1,0:T(8,128)(2,1)}, u32[]{:S(2)}) copy-start(bf16[512,256]{1,0:T(8,128)(2,1)} %param.33) | copy-start | bytes 786436
  140.8 22.2 %copy-start.6 = (bf16[128,2048]{1,0:T(8,128)(2,1)S(1)}, bf16[128,2048]{1,0:T(8,128)(2,1)}, u32[]{:S(2)}) copy-start(bf16[128,2048]{1,0:T(8,128)(2,1)} %param.29) | copy-start | bytes 1572868
  140.8 9.5 %all-to-all-start = ((bf16[4,128,256]{2,1,0:T(8,128)(2,1)}), bf16[4,128,256]{2,1,0:T(8,128)(2,1)S(1)}, u32[]{:S(2)}, u32[]{:S(2)}) async-start(bf16[4,128,256]{2,1,0:T(8,128)(2,1)} %bitcast.27), calls=%async_computation | async-start | bytes 524288 | tf_op jit(solution)/shard_map/all_to_all | solution.py:165
  150.3 9.6 %all-to-all-start.1 = ((bf16[4,128,256]{2,1,0:T(8,128)(2,1)}), bf16[4,128,256]{2,1,0:T(8,128)(2,1)S(1)}, u32[]{:S(2)}, u32[]{:S(2)}) async-start(bf16[4,128,256]{2,1,0:T(8,128)(2,1)} %bitcast.30), calls=%async_computation.1 | async-start | bytes 524288 | tf_op jit(solution)/shard_map/all_to_all | solution.py:166
  171.7 52.0 %copy-start.20 = (bf16[1,2048,1024]{2,1,0:T(8,128)(2,1)S(1)}, bf16[1,2048,1024]{2,1,0:T(8,128)(2,1)}, u32[]{:S(2)}) copy-start(bf16[1,2048,1024]{2,1,0:T(8,128)(2,1)} %param.49) | copy-start | bytes 12582916
  222.3 1.3 copy-start.3
  236.0 3.8 %copy-start.18 = (f32[128]{0:T(128)S(1)}, f32[128]{0:T(128)}, u32[]{:S(2)}) copy-start(f32[128]{0:T(128)} %param.47) | copy-start | bytes 1540
  236.0 3.8 %copy-start.19 = (f32[128]{0:T(128)S(1)}, f32[128]{0:T(128)}, u32[]{:S(2)}) copy-start(f32[128]{0:T(128)} %param.48) | copy-start | bytes 1540
  236.0 52.5 %all-to-all-start.3 = ((bf16[32,16,2048]{2,1,0:T(8,128)(2,1)}), bf16[32,16,2048]{2,1,0:T(8,128)(2,1)S(1)}, u32[]{:S(2)}, u32[]{:S(2)}) async-start(bf16[32,16,2048]{2,1,0:T(8,128)(2,1)} %bitcast.197), calls=%async_computation.3 | async-start | bytes 4194304 | tf_op jit(solution)/shard_map/all_to_all | solution.py:199
  290.8 5.2 %copy-start.1 = (bf16[4,64,64]{2,1,0:T(8,128)(2,1)S(1)}, bf16[4,64,64]{2,1,0:T(8,128)(2,1)}, u32[]{:S(2)}) copy-start(bf16[4,64,64]{2,1,0:T(8,128)(2,1)} %param.36) | copy-start | bytes 98308
Sparse Core Ops, SparseCore 0:
  8.9 37.1 all-gather.4
  47.7 34.4 all-gather.6
where the time goes:
time: 304 us; the launch traced here: 303 us
  blocking collectives  103 us (34%)
  waiting for transfers between devices  61.1 us (20%)
  other arithmetic  48.3 us (16%)
  matrix products  34.8 us (11%)
  local copies, waits for them, and re-layouts  21.6 us (7%)
  starting transfers between devices  19.4 us (6%)
  between operations  14.2 us (5%)
    all_gather x2, blocking collectives, prefix(): pieces = jax.tree.map(lambda part: lax.all_gather(part, axis), value)  52.2 us
    all_to_all x1, blocking collectives, shards(): lax.all_to_all(buffer, ('sp', 'tp'), split_axis=0, concat_axis=0, tiled=T...  50.7 us
    all_to_all x1, waiting for transfers between devices, shards(): lax.all_to_all(served.reshape(arrived.shape), ('sp', 'tp'), split_axis=0,...  48.6 us
    reduce_sum x4, other arithmetic, block_states(): return jnp.sum(weight * drive_block[None, :, :], axis=1)  39.1 us
    dot_general x1, matrix products, shards(): jnp.dot(inner, w_down[0], preferred_element_type=jnp.float32)  9.97 us
    ppermute x2, starting transfers between devices, from_behind(): return lax.ppermute(array, axis, pairs)  8.43 us
    dot_general x6, matrix products, causal_taps(): moved = jnp.dot(own_shift, source, preferred_element_type=jnp.float32)  8.2 us
  transfers between devices with their start and end apart: 7, of which 3 were waited for; matrix products, arithmetic and copies ran while one was open for 25% of the time, Pallas kernels for 0%

commit v1 on v0

v1 whole, which is shorter than its diff:
```python
import functools

import jax
import jax.numpy as jnp
from jax import lax
from jax.experimental import pallas as pl
from jax.experimental.pallas import tpu as pltpu
from jax.sharding import PartitionSpec as P

EPSILON = 1e-06
GATE_SCALE = 8.0
MESH = pl.DeviceIdType.MESH
VMEM_LIMIT = 60 * 1024 * 1024
RIM = 16


def greet(peers):
    barrier = pltpu.get_barrier_semaphore()
    for device in peers:
        pl.semaphore_signal(barrier, inc=1, device_id=device, device_id_type=MESH)
    pl.semaphore_wait(barrier, len(peers))


def front_kernel(
    sp_count, xa, xb, ga, gb, taps, gates, slope, jumps, hidden,
    padded, conv, gelu_out, factors, states, tail, ends, tail_send, tail_recv, end_send, end_recv,
):
    length, half = xa.shape
    width = 2 * half
    sp, tp = lax.axis_index("sp"), lax.axis_index("tp")

    def peer(k):
        return (lax.rem(sp + k, sp_count), tp)

    greet([peer(k) for k in range(1, sp_count)])
    copies = []
    for i, x in enumerate((xa, xb)):
        copy = pltpu.make_async_remote_copy(
            src_ref=x.at[pl.ds(length - RIM, RIM)], dst_ref=tail.at[i],
            send_sem=tail_send.at[i], recv_sem=tail_recv.at[i],
            device_id=peer(1), device_id_type=MESH,
        )
        copy.start()
        copies.append(copy)
    gelu_out[:, :half] = jax.nn.gelu(ga[...].astype(jnp.float32))
    gelu_out[:, half:] = jax.nn.gelu(gb[...].astype(jnp.float32))
    padded[RIM:, :half] = xa[...].astype(jnp.float32)
    padded[RIM:, half:] = xb[...].astype(jnp.float32)
    for copy in copies:
        copy.wait()
    keep = jnp.where(sp > 0, 1.0, 0.0).astype(jnp.float32)
    padded[:RIM, :half] = tail[0].astype(jnp.float32) * keep
    padded[:RIM, half:] = tail[1].astype(jnp.float32) * keep
    tap_count = taps.shape[0]
    total = jnp.zeros((length, width), jnp.float32)
    for offset in range(tap_count):
        lag = tap_count - 1 - offset
        total = total + taps[offset : offset + 1, :].astype(jnp.float32) * padded[pl.ds(RIM - lag, length), :]
    conv[...] = total.astype(jnp.bfloat16)
    block = gates.shape[1]
    for i in range(gates.shape[0]):
        span = slice(i * block, (i + 1) * block)
        c = conv[:, span]
        both = jnp.dot(c, gates[i], preferred_element_type=jnp.float32)
        recur = jax.nn.sigmoid(both[:, :block])
        admit = jax.nn.sigmoid(both[:, block:])
        log_decay = recur * slope[:, span] + jumps[...]
        factors[:, span] = jnp.exp(log_decay)
        y = 2.0 * log_decay
        series = -y * (1.0 + y * (1 / 2) * (1.0 + y * (1 / 3) * (1.0 + y * (1 / 4) * (1.0 + y * (1 / 5) * (1.0 + y * (1 / 6))))))
        gap = jnp.where(y > -0.25, series, 1.0 - jnp.exp(y))
        states[:, span] = jnp.sqrt(gap) * admit * c.astype(jnp.float32)
    group = 8
    row = lax.broadcasted_iota(jnp.int32, (group, width), 0)

    def link(g, carry):
        carry_factor, carry_state = carry
        at = pl.ds(pl.multiple_of(g * group, group), group)
        f, s = factors[at, :], states[at, :]
        shift = 1
        while shift < group:
            inside = row >= shift
            s = s + f * jnp.where(inside, pltpu.roll(s, shift, 0), 0.0)
            f = f * jnp.where(inside, pltpu.roll(f, shift, 0), 1.0)
            shift *= 2
        s = s + f * carry_state
        f = f * carry_factor
        factors[at, :] = f
        states[at, :] = s
        return f[group - 1 :, :], s[group - 1 :, :]

    one, zero = jnp.ones((1, width), jnp.float32), jnp.zeros((1, width), jnp.float32)
    last_factor, last_state = lax.fori_loop(0, length // group, link, (one, zero), unroll=8)
    ends[sp] = jnp.where(row == 0, last_factor, last_state)
    copies = []
    for k in range(1, sp_count):
        copy = pltpu.make_async_remote_copy(
            src_ref=ends.at[sp], dst_ref=ends.at[sp],
            send_sem=end_send.at[k], recv_sem=end_recv.at[k],
            device_id=peer(k), device_id_type=MESH,
        )
        copy.start()
        copies.append(copy)
    for copy in copies:
        copy.wait()

    def join(position, carried):
        longer = ends[position, 0:1, :] * carried + ends[position, 1:2, :]
        return jnp.where(position < sp, longer, carried)

    carried = lax.fori_loop(0, sp_count, join, zero)
    hidden[...] = ((states[...] + factors[...] * carried) * gelu_out[...]).astype(jnp.bfloat16)


def front(xa, xb, ga, gb, taps, gates, slope, jumps):
    sp_count = lax.axis_size("sp")
    length, half = xa.shape
    width = 2 * half
    vmem = pl.BlockSpec(memory_space=pltpu.VMEM)
    dma = pltpu.SemaphoreType.DMA
    return pl.pallas_call(
        functools.partial(front_kernel, sp_count),
        out_shape=jax.ShapeDtypeStruct((length, width), jnp.bfloat16),
        in_specs=[vmem] * 8,
        out_specs=vmem,
        scratch_shapes=[
            pltpu.VMEM((length + RIM, width), jnp.float32),
            pltpu.VMEM((length, width), jnp.bfloat16),
            pltpu.VMEM((length, width), jnp.float32),
            pltpu.VMEM((length, width), jnp.float32),
            pltpu.VMEM((length, width), jnp.float32),
            pltpu.VMEM((2, RIM, half), jnp.bfloat16),
            pltpu.VMEM((sp_count, 8, width), jnp.float32),
            dma((2,)), dma((2,)), dma((sp_count,)), dma((sp_count,)),
        ],
        compiler_params=pltpu.CompilerParams(
            collective_id=0, has_side_effects=True, vmem_limit_bytes=VMEM_LIMIT
        ),
    )(xa, xb, ga, gb, taps, gates, slope, jumps)


def mix_kernel(
    cuts, hidden, wa, wb, stream, gain, middle, normed,
    out_pair, in_pair, own, out_far, in_far, pair_send, pair_recv, far_send, far_recv,
):
    sp, tp = lax.axis_index("sp"), lax.axis_index("tp")
    rows = stream.shape[0]
    half = wa.shape[0]
    x, core = tp // 2, lax.rem(tp, 2)
    partner, across = (sp, x * 2 + 1 - core), (sp, (1 - x) * 2 + core)
    greet([partner, across])

    def part(owner):
        h = hidden[pl.ds(pl.multiple_of(owner * rows, rows), rows), :]
        return jnp.dot(h[:, :half], wa[...], preferred_element_type=jnp.float32) + jnp.dot(
            h[:, half:], wb[...], preferred_element_type=jnp.float32
        )

    pair = []
    for i, chip in enumerate((1 - x, x)):
        out_pair[i] = part(chip * 2 + 1 - core).astype(jnp.bfloat16)
        copy = pltpu.make_async_remote_copy(
            src_ref=out_pair.at[i], dst_ref=in_pair.at[i],
            send_sem=pair_send.at[i], recv_sem=pair_recv.at[i],
            device_id=partner, device_id_type=MESH,
        )
        copy.start()
        pair.append(copy)
    own[...] = part((1 - x) * 2 + core)
    pair[0].wait()
    step = rows // cuts
    far = []
    for j in range(cuts):
        span = pl.ds(j * step, step)
        out_far[span, :] = (own[span, :] + in_pair[0, span, :].astype(jnp.float32)).astype(jnp.bfloat16)
        copy = pltpu.make_async_remote_copy(
            src_ref=out_far.at[span], dst_ref=in_far.at[span],
            send_sem=far_send.at[j], recv_sem=far_recv.at[j],
            device_id=across, device_id_type=MESH,
        )
        copy.start()
        far.append(copy)
    own[...] = part(x * 2 + core)
    pair[1].wait()
    own[...] = own[...] + in_pair[1].astype(jnp.float32) + stream[...].astype(jnp.float32)
    for j in range(cuts):
        span = pl.ds(j * step, step)
        far[j].wait()
        m = (own[span, :] + in_far[span, :].astype(jnp.float32)).astype(jnp.bfloat16)
        middle[span, :] = m
        mf = m.astype(jnp.float32)
        scale = lax.rsqrt(jnp.mean(mf * mf, axis=-1, keepdims=True) + EPSILON)
        normed[span, :] = (mf * scale * gain[...].astype(jnp.float32)).astype(jnp.bfloat16)


def mix(hidden, wa, wb, stream, gain):
    rows, width = stream.shape
    cuts = 4
    vmem = pl.BlockSpec(memory_space=pltpu.VMEM)
    dma = pltpu.SemaphoreType.DMA
    shape = jax.ShapeDtypeStruct((rows, width), jnp.bfloat16)
    return pl.pallas_call(
        functools.partial(mix_kernel, cuts),
        out_shape=(shape, shape),
        in_specs=[vmem] * 5,
        out_specs=(vmem, vmem),
        scratch_shapes=[
            pltpu.VMEM((2, rows, width), jnp.bfloat16),
            pltpu.VMEM((2, rows, width), jnp.bfloat16),
            pltpu.VMEM((rows, width), jnp.float32),
            pltpu.VMEM((rows, width), jnp.bfloat16),
            pltpu.VMEM((rows, width), jnp.bfloat16),
            dma((2,)), dma((2,)), dma((cuts,)), dma((cuts,)),
        ],
        compiler_params=pltpu.CompilerParams(
            collective_id=1, has_side_effects=True, vmem_limit_bytes=VMEM_LIMIT
        ),
    )(hidden, wa, wb, stream, gain)


def pair_blocks(gate, block):
    heads, dim = gate.shape[0], gate.shape[1]
    join = block // dim
    if join == 1:
        return gate
    pieces = gate.reshape(heads // join, join, dim, dim)
    rows = [
        jnp.pad(pieces[:, i], ((0, 0), (0, 0), (i * dim, (join - 1 - i) * dim))) for i in range(join)
    ]
    return jnp.concatenate(rows, axis=1)


def shards(
    stream,
    conv_in_a,
    conv_in_b,
    gate_in_a,
    gate_in_b,
    conv_w_a,
    conv_w_b,
    rec_gate_a,
    inp_gate_a,
    rec_gate_b,
    inp_gate_b,
    decay_a,
    decay_b,
    decay_increments,
    out_w_a,
    out_w_b,
    norm_gain,
    expert_ids,
    group_prob,
    pick_gap,
    w_gate,
    w_up,
    w_down,
):
    block = max(rec_gate_a.shape[1], rec_gate_b.shape[1])
    recur = jnp.concatenate([pair_blocks(rec_gate_a, block), rec_gate_b], axis=0)
    admit = jnp.concatenate([pair_blocks(inp_gate_a, block), inp_gate_b], axis=0)
    gates = jnp.concatenate([recur, admit], axis=2)
    taps = jnp.concatenate([conv_w_a, conv_w_b], axis=1)
    slope = -GATE_SCALE * jax.nn.softplus(-jnp.concatenate([decay_a, decay_b]))[None, :]
    hidden = front(
        conv_in_a, conv_in_b, gate_in_a, gate_in_b, taps, gates, slope, decay_increments[:, None]
    )
    tp_count = lax.axis_size("tp")
    row_count = stream.shape[0]
    middle, normed = mix(hidden, out_w_a, out_w_b, stream, norm_gain[None, :])
    middle_f = middle.astype(jnp.float32)
    width = normed.shape[1]
    sequence_parallel_count = lax.axis_size("sp")
    experts = sequence_parallel_count * tp_count * w_gate.shape[0]
    slot_count = 4 * row_count // experts
    flat_ids = expert_ids.reshape(-1)
    onehot = (flat_ids[:, None] == jnp.arange(experts, dtype=jnp.int32)[None, :]).astype(jnp.int32)
    ranks = jnp.sum(jnp.cumsum(onehot, axis=0) * onehot, axis=1) - 1
    destination = flat_ids * slot_count + ranks
    copies = jnp.repeat(normed, expert_ids.shape[1], axis=0)
    buffer = jnp.zeros((experts * slot_count, width), jnp.bfloat16).at[destination].set(copies)
    buffer = buffer.reshape(experts, slot_count, width)
    arrived = lax.all_to_all(buffer, ("sp", "tp"), split_axis=0, concat_axis=0, tiled=True)
    flat_rows = arrived.reshape(-1, arrived.shape[-1])
    gate_part = jnp.dot(flat_rows, w_gate[0], preferred_element_type=jnp.float32)
    up_part = jnp.dot(flat_rows, w_up[0], preferred_element_type=jnp.float32)
    inner = (jax.nn.silu(gate_part) * up_part).astype(jnp.bfloat16)
    served = jnp.dot(inner, w_down[0], preferred_element_type=jnp.float32).astype(jnp.bfloat16)
    returned = lax.all_to_all(
        served.reshape(arrived.shape), ("sp", "tp"), split_axis=0, concat_axis=0, tiled=True
    )
    returned = returned.reshape(experts * slot_count, width)
    picked = returned[destination].reshape(row_count, expert_ids.shape[1], width)
    first_weight = group_prob * jax.nn.sigmoid(pick_gap)
    second_weight = group_prob * jax.nn.sigmoid(-pick_gap)
    total = (
        middle_f
        + first_weight[:, None] * picked[:, 0].astype(jnp.float32)
        + second_weight[:, None] * picked[:, 1].astype(jnp.float32)
    )
    return total.astype(jnp.bfloat16)


def solution(mesh):
    placed = (
        P(("sp", "tp"), None),
        P("sp", "tp"),
        P("sp", "tp"),
        P("sp", "tp"),
        P("sp", "tp"),
        P(None, "tp"),
        P(None, "tp"),
        P("tp", None, None),
        P("tp", None, None),
        P("tp", None, None),
        P("tp", None, None),
        P("tp"),
        P("tp"),
        P("sp"),
        P("tp", None),
        P("tp", None),
        P(),
        P(("sp", "tp"), None),
        P(("sp", "tp")),
        P(("sp", "tp")),
        P(("sp", "tp"), None, None),
        P(("sp", "tp"), None, None),
        P(("sp", "tp"), None, None),
    )
    return jax.shard_map(
        shards, mesh=mesh, in_specs=placed, out_specs=P(("sp", "tp"), None), check_vma=False
    )
```

time: 304 us -> 179 us (0.59)
  blocking collectives: 103 us -> 53.6 us
  other arithmetic: 48.3 us -> 7.57 us
  Pallas kernels: 0 us -> 37.5 us
  matrix products: 34.8 us -> 12.4 us
  starting transfers between devices: 19.4 us -> 3.65 us
  between operations: 14.2 us -> 0.18 us
  waiting for transfers between devices: 61.1 us -> 48.7 us
  local copies, waits for them, and re-layouts: 21.6 us -> 15 us
    all_gather x2 -> x0, blocking collectives: 52.2 us -> none  [prefix(): pieces = jax.tree.map(lambda part: lax.all_gather(part, axis), value)]
    reduce_sum x4 -> x0, other arithmetic: 39.1 us -> none  [block_states(): return jnp.sum(weight * drive_block[None, :, :], axis=1)]
    pallas_call x0 -> x2, Pallas kernels: none -> 37.5 us  [the longest x1 19.5 us: mix(): pl.pallas_call(functools.partial(mix_kernel, cuts), out_shape=(shape, sha...]
    dot_general x19 -> x0, matrix products: 22.5 us -> none  [the longest x6 8.2 us: causal_taps(): moved = jnp.dot(own_shift, source, preferred_element_type=jnp.float32)]
    all_to_all x2 -> x0, waiting for transfers between devices: 11.7 us -> none  [the longest x1 5.96 us: shards(): lax.all_to_all(hidden_a, 'tp', split_axis=0, concat_axis=1, tiled=True)]
    ppermute x2 -> x0, starting transfers between devices: 8.43 us -> none  [from_behind(): return lax.ppermute(array, axis, pairs)]
    all_to_all x2 -> x0, starting transfers between devices: 7.12 us -> none  [the longest x1 3.59 us: shards(): lax.all_to_all(hidden_b, 'tp', split_axis=0, concat_axis=1, tiled=True)]
    div x4 -> x0, local copies, waits for them, and re-layouts: 3.67 us -> none  [recurrence_inputs(): jax.nn.sigmoid(jnp.einsum('thi,hij->thj', blocks, rec_gate, preferred_ele...]
  transfers between devices with their start and end apart: 7 -> 1, of which waited for: 3 -> 1; matrix products, arithmetic and copies ran while one was open for 25% -> 0% of each run, Pallas kernels for 0% -> 0%
where the time goes in v1:
time: 179 us
  blocking collectives  53.6 us (30%)
  waiting for transfers between devices  48.7 us (27%)
  Pallas kernels  37.5 us (21%)
  local copies, waits for them, and re-layouts  15 us (8%)
  matrix products  12.4 us (7%)
  other arithmetic  7.57 us (4%)
  starting transfers between devices  3.65 us (2%)
    all_to_all x1, blocking collectives, shards(): lax.all_to_all(buffer, ('sp', 'tp'), split_axis=0, concat_axis=0, tiled=T...  53.6 us
    all_to_all x1, waiting for transfers between devices, shards(): lax.all_to_all(served.reshape(arrived.shape), ('sp', 'tp'), split_axis=0,...  48.7 us
    pallas_call x1, Pallas kernels, mix(): pl.pallas_call(functools.partial(mix_kernel, cuts), out_shape=(shape, sha...  19.5 us
    pallas_call x1, Pallas kernels, front(): pl.pallas_call(functools.partial(front_kernel, sp_count), out_shape=jax.S...  18.1 us
    dot_general x1, matrix products, shards(): jnp.dot(inner, w_down[0], preferred_element_type=jnp.float32)  10 us
    all_to_all x1, starting transfers between devices, shards(): lax.all_to_all(served.reshape(arrived.shape), ('sp', 'tp'), split_axis=0,...  3.65 us
  transfers between devices with their start and end apart: 1, of which 1 were waited for; matrix products, arithmetic and copies ran while one was open for 0% of the time, Pallas kernels for 0%

profile of v1, /device:TPU:0, one launch (start us, length us, event | category | flops | bytes accessed | tf_op | source)
XLA Modules:
  0.0 178.6 jit_solution(7961442092299327665)
XLA Ops:
  0.0 0.7 broadcast_multiply_fusion
  0.7 0.8 copy.30
  1.5 0.1 eq.25
  1.6 0.1 eq.29
  1.7 1.5 copy.28.jumps
  3.3 1.3 broadcast_in_dim.9.gain
  4.6 0.1 copy.29
  4.7 0.1 mul.60
  4.8 0.6 reduce-window.6
  5.4 0.2 slice_reduce_fusion
  5.7 0.1 fusion.42
  5.8 1.3 pad_maximum_fusion.taps
  7.1 0.8 slice_bitcast_fusion.1
  7.9 1.3 fusion.44.slope
  9.2 1.7 fusion.34.gates
  10.9 18.1 %shard_map.217.hidden = bf16[512,512]{1,0:T(8,128)(2,1)} custom-call(bf16[512,256]{1,0:T(8,128)(2,1)} %xa.1, bf16[512,256]{1,0:T(8,128)(2,1)} %xb.1, bf16[512,256]{1,0:T(8,128)(2,1)} %ga.1, bf16[512,256]{1,0:T(8,128)(2,1)} %gb.1, bf16[4,512]{1,0:T(4,128)(2,1)} %pad_maximum_fusion.taps, bf16[4,128,256]{2,1,0:T(8,128)(2,1)} %fusion.34.gates, ...), custom_call_target="tpu_custom_call" | custom-call | tf_op jit(solution)/shard_map/pallas_call | solution.py:121
  28.9 19.5 %shard_map.218 = (bf16[128,2048]{1,0:T(8,128)(2,1)}, bf16[128,2048]{1,0:T(8,128)(2,1)}) custom-call(bf16[512,512]{1,0:T(8,128)(2,1)} %shard_map.217.hidden, bf16[256,2048]{1,0:T(8,128)(2,1)} %wa.1, bf16[256,2048]{1,0:T(8,128)(2,1)} %wb.1, bf16[128,2048]{1,0:T(8,128)(2,1)} %stream.1, bf16[1,2048]{1,0:T(2,128)(2,1)} %broadcast_in_dim.9.gain), custom_call_target="tpu_custom_call" | custom-call | tf_op jit(solution)/shard_map/pallas_call | solution.py:202
  48.4 1.7 broadcast_in_dim.21
  50.1 0.4 reshape.161
  50.6 2.8 %scatter_custom_fusion = bf16[512,2048]{1,0:T(8,128)(2,1)S(1)} fusion(s32[256]{0:T(256)S(1)} %bitcast.76, bf16[256,2048]{1,0:T(8,128)(2,1)S(1)} %reshape.161, bf16[]{:T(256)} %constant.8.clone.1), kind=kCustom, calls=%fused_computation.15 | custom fusion | bytes 2097154 | tf_op jit(solution)/shard_map/scatter | solution.py:280
  53.4 0.0 copy-start.4
  53.4 53.6 %all_to_all.10 = bf16[32,16,2048]{2,1,0:T(8,128)(2,1)S(1)} all-to-all(bf16[32,16,2048]{2,1,0:T(8,128)(2,1)S(1)} %bitcast.70), channel_id=1, replica_groups=mesh['sp'=8,'tp'=4] {'sp','tp'}, dimensions={0} | all-to-all | bytes 4194304 | tf_op jit(solution)/shard_map/all_to_all | solution.py:282
  107.0 0.0 copy-start
  107.0 1.3 copy-done
  108.3 0.0 copy-done.4
  108.3 2.4 %fusion.4 = f32[512,1024]{1,0:T(8,128)S(1)} fusion(bf16[512,2048]{1,0:T(8,128)(2,1)S(1)} %bitcast.72, bf16[1,2048,1024]{2,1,0:T(8,128)(2,1)S(1)} %copy-done.4), kind=kOutput, calls=%fused_computation.6 | convolution fusion | flops 2147483648 | bytes 8388608 | tf_op jit(solution)/shard_map/dot_general | solution.py:284
  110.7 10.0 %fusion.6 = bf16[512,2048]{1,0:T(8,128)(2,1)} fusion(bf16[1,1024,2048]{2,1,0:T(8,128)(2,1)} %param.45, f32[512,1024]{1,0:T(8,128)S(1)} %fusion.4, bf16[512,2048]{1,0:T(8,128)(2,1)} %bitcast.73, bf16[1,2048,1024]{2,1,0:T(8,128)(2,1)} %param.44), kind=kOutput, calls=%fused_computation.8 | convolution fusion | flops 4299161600 | bytes 14680064 | tf_op jit(solution)/shard_map/dot_general | solution.py:287
  120.7 0.0 copy-start.2
  120.7 0.0 copy-start.3
  120.7 3.7 %all-to-all-start.1 = ((bf16[32,16,2048]{2,1,0:T(8,128)(2,1)}), bf16[32,16,2048]{2,1,0:T(8,128)(2,1)S(1)}, u32[]{:S(2)}, u32[]{:S(2)}) async-start(bf16[32,16,2048]{2,1,0:T(8,128)(2,1)} %bitcast.71), calls=%async_computation.1 | async-start | bytes 4194304 | tf_op jit(solution)/shard_map/all_to_all | solution.py:288
  124.4 0.0 copy-done.2
  124.4 0.0 copy-done.3
  124.4 48.7 %all-to-all-done.1 = bf16[32,16,2048]{2,1,0:T(8,128)(2,1)S(1)} async-done(((bf16[32,16,2048]{2,1,0:T(8,128)(2,1)}), bf16[32,16,2048]{2,1,0:T(8,128)(2,1)S(1)}, u32[]{:S(2)}, u32[]{:S(2)}) %all-to-all-start.1) | async-done | bytes 2097184 | tf_op jit(solution)/shard_map/all_to_all | solution.py:288
  173.1 1.4 gather_fusion
  174.5 0.7 reshape.146
  175.2 0.0 copy-start.1
  175.2 1.5 fusion.46
  176.7 0.0 copy-done.1
  176.7 1.9 %fusion.12 = bf16[128,2048]{1,0:T(8,128)(2,1)} fusion(bf16[128,2048]{1,0:T(8,128)(2,1)S(1)} %copy-done.1, bf16[128,1,2048]{2,1,0:T(2,128)(2,1)S(1)} %get-tuple-element.10, bf16[128,1,2048]{2,1,0:T(2,128)(2,1)S(1)} %get-tuple-element.9, f32[128]{0:T(128)S(1)} %get-tuple-element.16, f32[128]{0:T(128)S(1)} %get-tuple-element.15), kind=kLoop, calls=%fused_computation.12 | loop fusion | flops 2097152 | bytes 2098176 | tf_op jit(solution)/shard_map/convert_element_type | solution.py:300
  (7 shorter events, 0.1 us)
Async XLA Ops:
  53.4 54.9 %copy-start.4 = (bf16[1,2048,1024]{2,1,0:T(8,128)(2,1)S(1)}, bf16[1,2048,1024]{2,1,0:T(8,128)(2,1)}, u32[]{:S(2)}) copy-start(bf16[1,2048,1024]{2,1,0:T(8,128)(2,1)} %param.43) | copy-start | bytes 12582916
  107.0 1.4 copy-start
  120.7 3.7 %copy-start.2 = (f32[128]{0:T(128)S(1)}, f32[128]{0:T(128)}, u32[]{:S(2)}) copy-start(f32[128]{0:T(128)} %param.41) | copy-start | bytes 1540
  120.7 3.7 %copy-start.3 = (f32[128]{0:T(128)S(1)}, f32[128]{0:T(128)}, u32[]{:S(2)}) copy-start(f32[128]{0:T(128)} %param.42) | copy-start | bytes 1540
  120.7 52.4 %all-to-all-start.1 = ((bf16[32,16,2048]{2,1,0:T(8,128)(2,1)}), bf16[32,16,2048]{2,1,0:T(8,128)(2,1)S(1)}, u32[]{:S(2)}, u32[]{:S(2)}) async-start(bf16[32,16,2048]{2,1,0:T(8,128)(2,1)} %bitcast.71), calls=%async_computation.1 | async-start | bytes 4194304 | tf_op jit(solution)/shard_map/all_to_all | solution.py:288
  175.2 1.5 copy-start.1

commit v2 on v1

--- a/solution.py
+++ b/solution.py
@@ -9,6 +9,7 @@
 
 EPSILON = 1e-06
 GATE_SCALE = 8.0
+GROUPS = 4
 MESH = pl.DeviceIdType.MESH
 VMEM_LIMIT = 60 * 1024 * 1024
 RIM = 16
@@ -216,6 +217,242 @@
             collective_id=1, has_side_effects=True, vmem_limit_bytes=VMEM_LIMIT
         ),
     )(hidden, wa, wb, stream, gain)
+
+
+def seat(groups, size, tp_count):
+    me = lax.axis_index("sp") * tp_count + lax.axis_index("tp")
+    group, member = me // size, lax.rem(me, size)
+
+    def device(g, m):
+        flat = lax.rem(g, groups) * size + lax.rem(m, size)
+        return (flat // tp_count, lax.rem(flat, tp_count))
+
+    peers = [device(group, member + j) for j in range(1, size)]
+    peers += [device(group + k, member) for k in range(1, groups)]
+    return group, member, device, peers
+
+
+def near_first(groups):
+    return sorted(range(groups), key=lambda k: (min(k, groups - k), k))
+
+
+def spread_kernel(
+    tp_count, normed, place, meta, arrived, got_meta,
+    block, got, pieces, row_send, row_recv, meta_send, meta_recv, piece_send, piece_recv,
+):
+    groups, size, cap, width = arrived.shape
+    slots = place.shape[1]
+    group, member, device, peers = seat(groups, size, tp_count)
+    greet(peers)
+    order = near_first(groups)
+
+    def meta_copy(k):
+        return pltpu.make_async_remote_copy(
+            src_ref=meta.at[lax.rem(group + k, groups)], dst_ref=got_meta.at[group],
+            send_sem=meta_send.at[k], recv_sem=meta_recv.at[k],
+            device_id=device(group + k, member), device_id_type=MESH,
+        )
+
+    def row_copy(k):
+        return pltpu.make_async_remote_copy(
+            src_ref=block.at[lax.rem(group + k, groups)], dst_ref=got.at[group],
+            send_sem=row_send.at[k], recv_sem=row_recv.at[k],
+            device_id=device(group + k, member), device_id_type=MESH,
+        )
+
+    def piece_copy(k, j, to, origin):
+        source = lax.rem(group - k + groups, groups)
+        return pltpu.make_async_remote_copy(
+            src_ref=pieces.at[source, to], dst_ref=arrived.at[source, origin],
+            send_sem=piece_send.at[k, j], recv_sem=piece_recv.at[k, j],
+            device_id=device(group, to), device_id_type=MESH,
+        )
+
+    for k in order[1:]:
+        meta_copy(k).start()
+    for k in order[1:]:
+        to = lax.rem(group + k, groups)
+        block[to] = jnp.dot(place[to], normed[...], preferred_element_type=jnp.float32).astype(jnp.bfloat16)
+        row_copy(k).start()
+    got[group] = jnp.dot(place[group], normed[...], preferred_element_type=jnp.float32).astype(jnp.bfloat16)
+    got_meta[group] = meta[group]
+    slot = lax.broadcasted_iota(jnp.int32, (size * cap, slots), 0).astype(jnp.float32)
+    for k in order:
+        source = lax.rem(group - k + groups, groups)
+        if k:
+            meta_copy(k).wait_recv()
+            row_copy(k).wait_recv()
+        info = got_meta[source]
+        pick = jnp.where((slot == info[0:1, :slots]) | (slot == info[1:2, :slots]), 1.0, 0.0)
+        rows = jnp.dot(pick.astype(jnp.bfloat16), got[source], preferred_element_type=jnp.float32)
+        for e in range(size):
+            pieces[source, e] = rows[e * cap : (e + 1) * cap].astype(jnp.bfloat16)
+
+        def send(j, carry, k=k):
+            piece_copy(k, j, lax.rem(member + j, size), member).start()
+            return carry
+
+        lax.fori_loop(1, size, send, 0)
+        arrived[source, member] = pieces[source, member]
+    for k in order[1:]:
+        meta_copy(k).wait_send()
+        row_copy(k).wait_send()
+    for k in order:
+
+        def finish(j, carry, k=k):
+            piece_copy(k, j, lax.rem(member + j, size), lax.rem(member - j + size, size)).wait()
+            return carry
+
+        lax.fori_loop(1, size, finish, 0)
+
+
+def spread(normed, place, meta, size, cap):
+    groups, slots, _ = place.shape
+    width = normed.shape[1]
+    vmem = pl.BlockSpec(memory_space=pltpu.VMEM)
+    dma = pltpu.SemaphoreType.DMA
+    return pl.pallas_call(
+        functools.partial(spread_kernel, lax.axis_size("tp")),
+        out_shape=(
+            jax.ShapeDtypeStruct((groups, size, cap, width), jnp.bfloat16),
+            jax.ShapeDtypeStruct(meta.shape, meta.dtype),
+        ),
+        in_specs=[vmem] * 3,
+        out_specs=(vmem, vmem),
+        scratch_shapes=[
+            pltpu.VMEM((groups, slots, width), jnp.bfloat16),
+            pltpu.VMEM((groups, slots, width), jnp.bfloat16),
+            pltpu.VMEM((groups, size, cap, width), jnp.bfloat16),
+            dma((groups,)), dma((groups,)), dma((groups,)), dma((groups,)),
+            dma((groups, size)), dma((groups, size)),
+        ],
+        compiler_params=pltpu.CompilerParams(
+            collective_id=2, has_side_effects=True, vmem_limit_bytes=VMEM_LIMIT
+        ),
+    )(normed, place, meta)
+
+
+def collect_kernel(
+    tp_count, served, got_meta, middle, put, out,
+    held, outgoing, back, total, piece_send, piece_recv, row_send, row_recv,
+):
+    groups, size, cap, width = served.shape
+    slots = put.shape[2]
+    group, member, device, peers = seat(groups, size, tp_count)
+    greet(peers)
+    order = near_first(groups)[::-1]
+
+    def piece_copy(k, j, to, origin):
+        source = lax.rem(group - k + groups, groups)
+        return pltpu.make_async_remote_copy(
+            src_ref=served.at[source, to], dst_ref=held.at[source, origin],
+            send_sem=piece_send.at[k, j], recv_sem=piece_recv.at[k, j],
+            device_id=device(group, to), device_id_type=MESH,
+        )
+
+    def row_copy(k, origin):
+        return pltpu.make_async_remote_copy(
+            src_ref=outgoing.at[k], dst_ref=back.at[origin],
+            send_sem=row_send.at[k], recv_sem=row_recv.at[k],
+            device_id=device(group - k + groups, member), device_id_type=MESH,
+        )
+
+    for k in order:
+
+        def send(j, carry, k=k):
+            piece_copy(k, j, lax.rem(member + j, size), member).start()
+            return carry
+
+        lax.fori_loop(1, size, send, 0)
+    lane = lax.broadcasted_iota(jnp.int32, (slots, size * cap), 1).astype(jnp.float32)
+    total[...] = middle[...].astype(jnp.float32)
+    for k in order:
+        source = lax.rem(group - k + groups, groups)
+        held[source, member] = served[source, member]
+
+        def finish(j, carry, k=k):
+            piece_copy(k, j, lax.rem(member + j, size), lax.rem(member - j + size, size)).wait()
+            return carry
+
+        lax.fori_loop(1, size, finish, 0)
+        if cap % 16:
+            rows = jnp.concatenate(
+                [held[source, e].astype(jnp.float32) for e in range(size)], axis=0
+            ).astype(jnp.bfloat16)
+        else:
+            rows = held[source].reshape(size * cap, width)
+        info = got_meta[source].T[:slots]
+        first = jnp.dot(
+            jnp.where(info[:, 0:1] == lane, 1.0, 0.0).astype(jnp.bfloat16), rows,
+            preferred_element_type=jnp.float32,
+        )
+        second = jnp.dot(
+            jnp.where(info[:, 1:2] == lane, 1.0, 0.0).astype(jnp.bfloat16), rows,
+            preferred_element_type=jnp.float32,
+        )
+        joined = (info[:, 2:3] * first + info[:, 3:4] * second).astype(jnp.bfloat16)
+        if k:
+            outgoing[k] = joined
+            row_copy(k, group).start()
+        else:
+            total[...] += jnp.dot(put[group], joined, preferred_element_type=jnp.float32)
+    for k in order:
+        if k:
+            origin = lax.rem(group + k, groups)
+            row_copy(k, origin).wait()
+            total[...] += jnp.dot(put[origin], back[origin], preferred_element_type=jnp.float32)
+    out[...] = total[...].astype(jnp.bfloat16)
+
+
+def collect(served, got_meta, middle, put):
+    groups, size, cap, width = served.shape
+    slots = put.shape[2]
+    vmem = pl.BlockSpec(memory_space=pltpu.VMEM)
+    dma = pltpu.SemaphoreType.DMA
+    return pl.pallas_call(
+        functools.partial(collect_kernel, lax.axis_size("tp")),
+        out_shape=jax.ShapeDtypeStruct(middle.shape, jnp.bfloat16),
+        in_specs=[vmem] * 4,
+        out_specs=vmem,
+        scratch_shapes=[
+            pltpu.VMEM((groups, size, cap, width), jnp.bfloat16),
+            pltpu.VMEM((groups, slots, width), jnp.bfloat16),
+            pltpu.VMEM((groups, slots, width), jnp.bfloat16),
+            pltpu.VMEM(middle.shape, jnp.float32),
+            dma((groups, size)), dma((groups, size)), dma((groups,)), dma((groups,)),
+        ],
+        compiler_params=pltpu.CompilerParams(
+            collective_id=3, has_side_effects=True, vmem_limit_bytes=VMEM_LIMIT
+        ),
+    )(served, got_meta, middle, put)
+
+
+def routes(expert_ids, group_prob, pick_gap, experts, cap):
+    row_count = expert_ids.shape[0]
+    size = experts // GROUPS
+    slots = size * cap // 2
+    flat_ids = expert_ids.reshape(-1)
+    onehot = (flat_ids[:, None] == jnp.arange(experts, dtype=jnp.int32)[None, :]).astype(jnp.int32)
+    ranks = (jnp.sum(jnp.cumsum(onehot, axis=0) * onehot, axis=1) - 1).reshape(row_count, -1)
+    positions = ((expert_ids % size) * cap + ranks + 1).astype(jnp.float32)
+    group = expert_ids[:, 0] // size
+    mine = (group[:, None] == jnp.arange(GROUPS, dtype=jnp.int32)[None, :]).astype(jnp.int32)
+    slot = group * slots + jnp.sum(jnp.cumsum(mine, axis=0) * mine, axis=1) - 1
+    index = jnp.arange(GROUPS * slots, dtype=jnp.int32)
+    hit = index[:, None] == slot[None, :]
+    place = hit.astype(jnp.bfloat16).reshape(GROUPS, slots, row_count)
+    values = jnp.stack([
+        positions[:, 0],
+        positions[:, 1],
+        group_prob * jax.nn.sigmoid(pick_gap),
+        group_prob * jax.nn.sigmoid(-pick_gap),
+    ])
+    spots = jnp.sum(jnp.where(hit[None], values[:, None, :], 0.0), axis=2)
+    spots = spots - jnp.array([1.0, 1.0, 0.0, 0.0], jnp.float32)[:, None]
+    spots = jnp.transpose(spots.reshape(4, GROUPS, slots), (1, 0, 2))
+    lanes = -(-slots // 128) * 128
+    meta = jnp.pad(spots, ((0, 0), (0, 4), (0, lanes - slots)))
+    return place, jnp.transpose(place, (0, 2, 1)), meta
 
 
 def pair_blocks(gate, block):
@@ -267,37 +504,16 @@
     tp_count = lax.axis_size("tp")
     row_count = stream.shape[0]
     middle, normed = mix(hidden, out_w_a, out_w_b, stream, norm_gain[None, :])
-    middle_f = middle.astype(jnp.float32)
-    width = normed.shape[1]
-    sequence_parallel_count = lax.axis_size("sp")
-    experts = sequence_parallel_count * tp_count * w_gate.shape[0]
-    slot_count = 4 * row_count // experts
-    flat_ids = expert_ids.reshape(-1)
-    onehot = (flat_ids[:, None] == jnp.arange(experts, dtype=jnp.int32)[None, :]).astype(jnp.int32)
-    ranks = jnp.sum(jnp.cumsum(onehot, axis=0) * onehot, axis=1) - 1
-    destination = flat_ids * slot_count + ranks
-    copies = jnp.repeat(normed, expert_ids.shape[1], axis=0)
-    buffer = jnp.zeros((experts * slot_count, width), jnp.bfloat16).at[destination].set(copies)
-    buffer = buffer.reshape(experts, slot_count, width)
-    arrived = lax.all_to_all(buffer, ("sp", "tp"), split_axis=0, concat_axis=0, tiled=True)
+    experts = lax.axis_size("sp") * tp_count * w_gate.shape[0]
+    cap = 4 * row_count // experts
+    place, put, meta = routes(expert_ids, group_prob, pick_gap, experts, cap)
+    arrived, got_meta = spread(normed, place, meta, experts // GROUPS, cap)
     flat_rows = arrived.reshape(-1, arrived.shape[-1])
     gate_part = jnp.dot(flat_rows, w_gate[0], preferred_element_type=jnp.float32)
     up_part = jnp.dot(flat_rows, w_up[0], preferred_element_type=jnp.float32)
     inner = (jax.nn.silu(gate_part) * up_part).astype(jnp.bfloat16)
     served = jnp.dot(inner, w_down[0], preferred_element_type=jnp.float32).astype(jnp.bfloat16)
-    returned = lax.all_to_all(
-        served.reshape(arrived.shape), ("sp", "tp"), split_axis=0, concat_axis=0, tiled=True
-    )
-    returned = returned.reshape(experts * slot_count, width)
-    picked = returned[destination].reshape(row_count, expert_ids.shape[1], width)
-    first_weight = group_prob * jax.nn.sigmoid(pick_gap)
-    second_weight = group_prob * jax.nn.sigmoid(-pick_gap)
-    total = (
-        middle_f
-        + first_weight[:, None] * picked[:, 0].astype(jnp.float32)
-        + second_weight[:, None] * picked[:, 1].astype(jnp.float32)
-    )
-    return total.astype(jnp.bfloat16)
+    return collect(served.reshape(arrived.shape), got_meta, middle, put)
 
 
 def solution(mesh):

time: 179 us -> 147 us (0.82)
  Pallas kernels: 37.5 us -> 113 us
  blocking collectives: 53.6 us -> 0 us
  waiting for transfers between devices: 48.7 us -> 0 us
  local copies, waits for them, and re-layouts: 15 us -> 7.31 us
  matrix products: 12.4 us -> 16.6 us
  starting transfers between devices: 3.65 us -> 0 us
    pallas_call x0 -> x2, Pallas kernels: none -> 75.9 us  [the longest x1 38.5 us: collect(): pl.pallas_call(functools.partial(collect_kernel, lax.axis_size('tp')), ou...]
    all_to_all x1 -> x0, blocking collectives: 53.6 us -> none  [shards(): lax.all_to_all(buffer, ('sp', 'tp'), split_axis=0, concat_axis=0, tiled=T...]
    all_to_all x1 -> x0, waiting for transfers between devices: 48.7 us -> none  [shards(): lax.all_to_all(served.reshape(arrived.shape), ('sp', 'tp'), split_axis=0,...]
    dot_general x1, matrix products: 2.36 us -> 6.59 us  [shards(): jnp.dot(flat_rows, w_gate[0], preferred_element_type=jnp.float32)]
    all_to_all x1 -> x0, starting transfers between devices: 3.65 us -> none  [shards(): lax.all_to_all(served.reshape(arrived.shape), ('sp', 'tp'), split_axis=0,...]
    scatter x1 -> x0, local copies, waits for them, and re-layouts: 2.82 us -> none  [shards(): jnp.zeros((experts * slot_count, width), jnp.bfloat16).at[destination]]
  transfers between devices with their start and end apart: 1 -> 0, of which waited for: 1 -> 0; matrix products, arithmetic and copies ran while one was open for 0% -> 0% of each run, Pallas kernels for 0% -> 0%
where the time goes in v2:
time: 147 us
  Pallas kernels  113 us (77%)
  matrix products  16.6 us (11%)
  other arithmetic  9.31 us (6%)
  local copies, waits for them, and re-layouts  7.31 us (5%)
    pallas_call x1, Pallas kernels, collect(): pl.pallas_call(functools.partial(collect_kernel, lax.axis_size('tp')), ou...  38.5 us
    pallas_call x1, Pallas kernels, spread(): pl.pallas_call(functools.partial(spread_kernel, lax.axis_size('tp')), out...  37.4 us
    pallas_call x1, Pallas kernels, mix(): pl.pallas_call(functools.partial(mix_kernel, cuts), out_shape=(shape, sha...  19.5 us
    pallas_call x1, Pallas kernels, front(): pl.pallas_call(functools.partial(front_kernel, sp_count), out_shape=jax.S...  18.1 us
    dot_general x1, matrix products, shards(): jnp.dot(inner, w_down[0], preferred_element_type=jnp.float32)  9.99 us
    dot_general x1, matrix products, shards(): jnp.dot(flat_rows, w_gate[0], preferred_element_type=jnp.float32)  6.59 us

profile of v2, /device:TPU:0, one launch (start us, length us, event | category | flops | bytes accessed | tf_op | source)
XLA Modules:
  0.0 146.8 jit_solution(8739415123574466189)
XLA Ops:
  0.0 0.0 copy-start.2
  0.0 0.0 copy-start.1
  0.0 0.0 copy-start.4
  0.0 0.0 copy-start.3
  0.0 0.8 copy.59
  0.8 0.1 eq.100
  1.0 0.6 reduce-window.6
  1.6 0.0 copy-start
  1.6 0.2 slice_reduce_fusion.2
  1.8 0.1 eq.96
  2.0 0.1 fusion.43
  2.1 0.1 sub.31
  2.2 0.7 broadcast_compare_fusion
  2.9 0.1 copy.62
  3.1 0.2 slice_reduce_fusion.1
  3.3 0.7 fusion.48
  4.0 0.7 fusion.47
  4.7 0.1 fusion.41
  4.8 0.2 reduce_window_sum.26
  4.9 0.2 select_reduce_fusion.1
  5.1 0.7 add_add_fusion
  5.8 0.2 select_reduce_fusion
  6.1 0.1 reduce_sum.32
  6.1 0.7 fusion.45
  6.9 0.6 pad.22.meta
  7.5 0.8 slice_bitcast_fusion.1
  8.3 1.7 %fusion.29.gates = bf16[4,128,256]{2,1,0:T(8,128)(2,1)} fusion(bf16[2,64,64]{2,1,0:T(8,128)(2,1)S(1)} %get-tuple-element.18, bf16[2,64,64]{2,1,0:T(8,128)(2,1)S(1)} %get-tuple-element.17, bf16[2,64,64]{2,1,0:T(8,128)(2,1)S(1)} %get-tuple-element.21, bf16[2,64,64]{2,1,0:T(8,128)(2,1)S(1)} %get-tuple-element.22, bf16[2,128,128]{2,1,0:T(8,128)(2,1)} %param.34, ...), kind=kLoop, calls=%fused_computation.30 | loop fusion | flops 4587520 | bytes 458752 | tf_op jit(solution)/shard_map/concatenate | solution.py:498
  10.0 1.5 %copy.57.jumps = f32[512,1]{1,0:T(8,128)} copy(f32[512,1]{0,1:T(1,128)} %bitcast.78) | data formatting | bytes 4096 | tf_op jit(solution)/shard_map/broadcast_in_dim | solution.py:502
  11.5 0.0 copy-done.2
  11.5 0.0 copy-done.1
  11.5 0.6 pad_maximum_fusion.taps
  12.1 0.0 copy-done.4
  12.1 0.0 copy-done.3
  12.1 0.6 fusion.46.slope
  12.7 18.1 %shard_map.226.hidden = bf16[512,512]{1,0:T(8,128)(2,1)} custom-call(bf16[512,256]{1,0:T(8,128)(2,1)} %xa.1, bf16[512,256]{1,0:T(8,128)(2,1)} %xb.1, bf16[512,256]{1,0:T(8,128)(2,1)} %ga.1, bf16[512,256]{1,0:T(8,128)(2,1)} %gb.1, bf16[4,512]{1,0:T(4,128)(2,1)} %pad_maximum_fusion.taps, bf16[4,128,256]{2,1,0:T(8,128)(2,1)} %fusion.29.gates, ...), custom_call_target="tpu_custom_call" | custom-call | tf_op jit(solution)/shard_map/pallas_call | solution.py:122
  30.8 0.0 copy-done
  30.8 0.6 broadcast_in_dim.36.gain
  31.4 19.5 %shard_map.227 = (bf16[128,2048]{1,0:T(8,128)(2,1)}, bf16[128,2048]{1,0:T(8,128)(2,1)}) custom-call(bf16[512,512]{1,0:T(8,128)(2,1)} %shard_map.226.hidden, bf16[256,2048]{1,0:T(8,128)(2,1)} %wa.1, bf16[256,2048]{1,0:T(8,128)(2,1)} %wb.1, bf16[128,2048]{1,0:T(8,128)(2,1)} %stream.1, bf16[1,2048]{1,0:T(2,128)(2,1)} %broadcast_in_dim.36.gain), custom_call_target="tpu_custom_call" | custom-call | tf_op jit(solution)/shard_map/pallas_call | solution.py:203
  50.9 0.7 compare_convert_fusion.1.place
  51.6 37.4 %shard_map.228 = (bf16[4,8,16,2048]{3,2,1,0:T(8,128)(2,1)}, f32[4,8,128]{2,1,0:T(8,128)}) custom-call(bf16[128,2048]{1,0:T(8,128)(2,1)} %get-tuple-element.9.normed, bf16[4,64,128]{2,1,0:T(8,128)(2,1)} %compare_convert_fusion.1.place, f32[4,8,128]{2,1,0:T(8,128)} %pad.22.meta), custom_call_target="tpu_custom_call" | custom-call | tf_op jit(solution)/shard_map/pallas_call | solution.py:314
  89.0 0.0 copy-start.5
  89.1 6.6 %fusion.4 = f32[512,1024]{1,0:T(8,128)} fusion(bf16[512,2048]{1,0:T(8,128)(2,1)} %bitcast.83, bf16[1,2048,1024]{2,1,0:T(8,128)(2,1)} %param.44), kind=kOutput, calls=%fused_computation.4 | convolution fusion | flops 2147483648 | bytes 8388608 | tf_op jit(solution)/shard_map/dot_general | solution.py:512
  95.7 0.0 copy-done.5
  95.7 10.0 %fusion.6 = bf16[512,2048]{1,0:T(8,128)(2,1)} fusion(bf16[1,1024,2048]{2,1,0:T(8,128)(2,1)} %param.46, f32[512,1024]{1,0:T(8,128)} %fusion.4, bf16[512,2048]{1,0:T(8,128)(2,1)S(1)} %bitcast.84, bf16[1,2048,1024]{2,1,0:T(8,128)(2,1)} %param.45), kind=kOutput, calls=%fused_computation.6 | convolution fusion | flops 4299161600 | bytes 14680064 | tf_op jit(solution)/shard_map/dot_general | solution.py:515
  105.6 0.7 compare_convert_fusion.put
  106.4 38.5 %shard_map.229 = bf16[128,2048]{1,0:T(8,128)(2,1)} custom-call(bf16[4,8,16,2048]{3,2,1,0:T(8,128)(2,1)} %bitcast.75, f32[4,8,128]{2,1,0:T(8,128)} %get-tuple-element.11.got_meta, bf16[128,2048]{1,0:T(8,128)(2,1)} %get-tuple-element.12.middle, bf16[4,128,64]{2,1,0:T(8,128)(2,1)} %compare_convert_fusion.put), custom_call_target="tpu_custom_call" | custom-call | tf_op jit(solution)/shard_map/pallas_call | solution.py:412
  144.9 1.9 %copy.82 = bf16[128,2048]{1,0:T(8,128)(2,1)} copy(bf16[128,2048]{1,0:T(8,128)(2,1)} %shard_map.229) | data formatting | bytes 1048576
  (8 shorter events, 0.1 us)
Async XLA Ops:
  0.0 11.5 %copy-start.2 = (bf16[4,256]{1,0:T(4,128)(2,1)S(1)}, bf16[4,256]{1,0:T(4,128)(2,1)}, u32[]{:S(2)}) copy-start(bf16[4,256]{1,0:T(4,128)(2,1)} %param.29) | copy-start | bytes 6148
  0.0 11.5 %copy-start.1 = (bf16[4,256]{1,0:T(4,128)(2,1)S(1)}, bf16[4,256]{1,0:T(4,128)(2,1)}, u32[]{:S(2)}) copy-start(bf16[4,256]{1,0:T(4,128)(2,1)} %param.30) | copy-start | bytes 6148
  0.0 12.1 %copy-start.4 = (f32[256]{0:T(256)S(1)}, f32[256]{0:T(256)}, u32[]{:S(2)}) copy-start(f32[256]{0:T(256)} %param.35) | copy-start | bytes 3076
  0.0 12.1 %copy-start.3 = (f32[256]{0:T(256)S(1)}, f32[256]{0:T(256)}, u32[]{:S(2)}) copy-start(f32[256]{0:T(256)} %param.36) | copy-start | bytes 3076
  1.6 29.2 %copy-start = (bf16[2048]{0:T(1024)(128)(2,1)S(1)}, bf16[2048]{0:T(1024)(128)(2,1)}, u32[]{:S(2)}) copy-start(bf16[2048]{0:T(1024)(128)(2,1)} %param.40) | copy-start | bytes 12292
  89.0 6.6 %copy-start.5 = (bf16[4,8,16,2048]{3,2,1,0:T(8,128)(2,1)S(1)}, bf16[4,8,16,2048]{3,2,1,0:T(8,128)(2,1)}, u32[]{:S(2)}) copy-start(bf16[4,8,16,2048]{3,2,1,0:T(8,128)(2,1)} %get-tuple-element.10) | copy-start | bytes 6291460
